TPU v7x, 32 devices: a whole 2x2x4 slice. The times are simulated.
32 devices in a mesh: tp: 16 (over z, y, x), dp: 2 (over core).
Axes of the slice: x: 2, y: 2, z: 4, core: 2. Of those that a mesh axis runs over, the one named last changes fastest.
Arguments:
- hidden: bfloat16 [16, 4096], P(None, 'dp'), may hold values from -6 to 6
- norm_gain: float32 [2, 4096], P(None, 'dp'), may hold values from 0.1 to 1.9
- gate_weight: bfloat16 [2, 4096, 8192], P(None, 'dp', 'tp'), may hold values from -0.09375 to 0.09375
- inner_weight: bfloat16 [2, 4096, 8192], P(None, 'dp', 'tp'), may hold values from -0.09375 to 0.09375
- write_weight: bfloat16 [2, 4096, 2048], P(None, 'dp', 'tp'), may hold values from -0.09375 to 0.09375
- read_weight: bfloat16 [2, 4096, 2048], P(None, 'dp', 'tp'), may hold values from -0.09375 to 0.09375
- step_weight: bfloat16 [2, 4096, 128], P(None, 'dp'), may hold values from -0.09375 to 0.09375
- conv_inner: bfloat16 [2, 4, 8192], P(None, None, 'tp'), may hold values from -3 to 3
- conv_write: bfloat16 [2, 4, 2048], P(None, None, 'tp'), may hold values from -3 to 3
- conv_read: bfloat16 [2, 4, 2048], P(None, None, 'tp'), may hold values from -3 to 3
- step_bias: float32 [2, 128], P(None, 'tp'), may hold values from -4 to -1
- decay_log: float32 [2, 128], P(None, 'tp'), may hold values from -3 to 0.5
- skip_gain: float32 [2, 128], P(None, 'tp'), may hold values from 0.1 to 1.9
- group_gain: float32 [2, 8192], P(None, 'tp'), may hold values from 0.1 to 1.9
- out_weight: bfloat16 [2, 8192, 4096], P(None, 'tp', 'dp'), may hold values from -0.4 to 0.4
- state_inner: bfloat16 [2, 16, 3, 8192], P(None, 'dp', None, 'tp'), may hold values from -6 to 6
- state_write: bfloat16 [2, 16, 3, 2048], P(None, 'dp', None, 'tp'), may hold values from -6 to 6
- state_read: bfloat16 [2, 16, 3, 2048], P(None, 'dp', None, 'tp'), may hold values from -6 to 6
- recurrent: float32 [2, 16, 128, 64, 128], P(None, 'dp', 'tp'), may hold values from -1.2 to 1.2, as said below
Outputs:
- out_hidden: bfloat16 [16, 4096], P(None, 'dp')
- next_inner: bfloat16 [2, 16, 3, 8192], P(None, 'dp', None, 'tp')
- next_write: bfloat16 [2, 16, 3, 2048], P(None, 'dp', None, 'tp')
- next_read: bfloat16 [2, 16, 3, 2048], P(None, 'dp', None, 'tp')
- next_recurrent: float32 [2, 16, 128, 64, 128], P(None, 'dp', 'tp')
Inputs may be any that keep to these rules, and one draw needn't show every extreme that they name: recurrent states of order a tenth, with scales that differ between heads.
All inputs are finite; a program needn't handle non-finite values.
Results may differ from a plain program's by a relative error of at most 0.025.
Values may be sent and summed in bfloat16 or wider, within the bound.
A program may use at most 64 MiB of HBM per device.

v0:
```python
import jax
import jax.numpy as jnp
from jax import lax
from jax.sharding import PartitionSpec as P

D = 4096
HEADS = 128
GROUPS = 16
eps = 1e-06


def convolve(state, fresh_row, kernel):
    window = jnp.concatenate([state, fresh_row[:, None, :]], axis=1)
    summed = jnp.sum(window.astype(jnp.float32) * kernel.astype(jnp.float32)[None], axis=1)
    return (jax.nn.silu(summed), window[:, 1:])


def mixer_block(normed, number, weights):
    (
        gate_weight,
        inner_weight,
        write_weight,
        read_weight,
        step_weight,
        conv_inner,
        conv_write,
        conv_read,
        step_bias,
        decay_log,
        skip_gain,
        group_gain,
        out_weight,
        state_inner,
        state_write,
        state_read,
        recurrent,
    ) = weights

    def partial_of(weight):
        return jnp.dot(normed, weight[number], preferred_element_type=jnp.float32).astype(
            jnp.bfloat16
        )

    summed = (
        lax.psum_scatter(partial_of(gate_weight), "dp", scatter_dimension=0, tiled=True).astype(
            jnp.float32
        ),
        lax.psum_scatter(partial_of(inner_weight), "dp", scatter_dimension=0, tiled=True).astype(
            jnp.float32
        ),
        lax.psum_scatter(partial_of(write_weight), "dp", scatter_dimension=0, tiled=True).astype(
            jnp.float32
        ),
        lax.psum_scatter(partial_of(read_weight), "dp", scatter_dimension=0, tiled=True).astype(
            jnp.float32
        ),
        lax.psum_scatter(partial_of(step_weight), "dp", scatter_dimension=0, tiled=True).astype(
            jnp.float32
        ),
    )
    gate_raw, inner_raw, write_raw, read_raw, step_raw = [
        member.astype(jnp.bfloat16) for member in summed
    ]
    inner_act, next_inner = convolve(state_inner[number], inner_raw, conv_inner[number])
    write_act, next_write = convolve(state_write[number], write_raw, conv_write[number])
    read_act, next_read = convolve(state_read[number], read_raw, conv_read[number])
    write_all, read_all = (
        lax.all_gather(write_act.astype(jnp.bfloat16), "tp", axis=1, tiled=True),
        lax.all_gather(read_act.astype(jnp.bfloat16), "tp", axis=1, tiled=True),
    )
    heads_here = step_bias.shape[1]
    head_dim = recurrent.shape[3]
    state_dim = recurrent.shape[4]
    rows_here = inner_act.shape[0]
    first_head = lax.axis_index("tp") * heads_here
    group_index = first_head // (HEADS // GROUPS)
    write_grid = write_all.reshape(rows_here, state_dim, GROUPS)
    read_grid = read_all.reshape(rows_here, state_dim, GROUPS)
    write_vec = lax.dynamic_slice_in_dim(write_grid, group_index, 1, 2)[:, :, 0].astype(jnp.float32)
    read_vec = lax.dynamic_slice_in_dim(read_grid, group_index, 1, 2)[:, :, 0].astype(jnp.float32)
    step_own = lax.dynamic_slice_in_dim(step_raw, first_head, heads_here, 1)
    step_size = jax.nn.softplus(step_own.astype(jnp.float32) + step_bias[number][None, :])
    retain = jnp.exp(-step_size * jnp.exp(decay_log[number])[None, :])
    inner_heads = inner_act.reshape(rows_here, heads_here, head_dim)
    updated = (
        retain[:, :, None, None] * recurrent[number]
        + (step_size[:, :, None] * inner_heads)[:, :, :, None] * write_vec[:, None, None, :]
    )
    readout = jnp.einsum("bhpn,bn->bhp", updated, read_vec, precision=lax.Precision.HIGHEST)
    readout = readout + skip_gain[number][None, :, None] * inner_heads
    gated_out = readout.reshape(rows_here, heads_here * head_dim) * jax.nn.silu(
        gate_raw.astype(jnp.float32)
    )
    selector = (jnp.arange(GROUPS) == group_index).astype(jnp.float32)
    totals = lax.psum(jnp.sum(gated_out * gated_out, axis=1)[:, None] * selector[None, :], "tp")
    group_sum = jnp.sum(totals * selector[None, :], axis=1, keepdims=True)
    group_factor = lax.rsqrt(group_sum / (HEADS // GROUPS * head_dim) + eps)
    group_normed = (gated_out * group_factor * group_gain[number][None, :]).astype(jnp.bfloat16)
    branch = jnp.dot(
        lax.all_gather(group_normed, "dp", axis=0, tiled=True),
        out_weight[number],
        preferred_element_type=jnp.float32,
    )
    return (branch, (next_inner, next_write, next_read, updated))


def total_over(branch):
    return lax.psum(branch, "tp")


def local(
    hidden,
    norm_gain,
    gate_weight,
    inner_weight,
    write_weight,
    read_weight,
    step_weight,
    conv_inner,
    conv_write,
    conv_read,
    step_bias,
    decay_log,
    skip_gain,
    group_gain,
    out_weight,
    state_inner,
    state_write,
    state_read,
    recurrent,
):
    weights = (
        gate_weight,
        inner_weight,
        write_weight,
        read_weight,
        step_weight,
        conv_inner,
        conv_write,
        conv_read,
        step_bias,
        decay_log,
        skip_gain,
        group_gain,
        out_weight,
        state_inner,
        state_write,
        state_read,
        recurrent,
    )
    wide_in = hidden.astype(jnp.float32)
    squares = lax.psum(jnp.sum(wide_in * wide_in, axis=1, keepdims=True), "dp")
    normed = (wide_in * lax.rsqrt(squares / D + eps) * norm_gain[0][None, :]).astype(jnp.bfloat16)
    branch, first_states = mixer_block(normed, 0, weights)
    middle = (wide_in + total_over(branch)).astype(jnp.bfloat16).astype(jnp.float32)
    squares = lax.psum(jnp.sum(middle * middle, axis=1, keepdims=True), "dp")
    normed = (middle * lax.rsqrt(squares / D + eps) * norm_gain[1][None, :]).astype(jnp.bfloat16)
    branch, second_states = mixer_block(normed, 1, weights)
    result = (middle + total_over(branch)).astype(jnp.bfloat16)
    stacked = [jnp.stack([earlier, later]) for earlier, later in zip(first_states, second_states)]
    return (result, stacked[0], stacked[1], stacked[2], stacked[3])


def solution(mesh):
    return jax.shard_map(
        local,
        mesh=mesh,
        in_specs=(
            P(None, "dp"),
            P(None, "dp"),
            P(None, "dp", "tp"),
            P(None, "dp", "tp"),
            P(None, "dp", "tp"),
            P(None, "dp", "tp"),
            P(None, "dp", None),
            P(None, None, "tp"),
            P(None, None, "tp"),
            P(None, None, "tp"),
            P(None, "tp"),
            P(None, "tp"),
            P(None, "tp"),
            P(None, "tp"),
            P(None, "tp", "dp"),
            P(None, "dp", None, "tp"),
            P(None, "dp", None, "tp"),
            P(None, "dp", None, "tp"),
            P(None, "dp", "tp", None, None),
        ),
        out_specs=(
            P(None, "dp"),
            P(None, "dp", None, "tp"),
            P(None, "dp", None, "tp"),
            P(None, "dp", None, "tp"),
            P(None, "dp", "tp", None, None),
        ),
        check_vma=False,
    )
```

profile of v0, /device:TPU:0, one launch (start us, length us, event | category | flops | bytes accessed | tf_op | source)
XLA Modules:
  0.0 509.0 jit_solution(9227752754220769065)
XLA Ops:
  7.2 1.0 fusion.58
  8.2 2.6 psum.42
  10.8 0.8 fusion.97
  11.8 2.8 fusion.28
  14.7 2.6 fusion.31
  17.4 0.6 dynamic-slice
  18.8 0.2 convolution_convert_fusion.4
  19.1 0.2 convolution_convert_fusion.3
  19.3 1.3 convolution_convert_fusion.5
  20.6 3.5 all-reduce.7
  24.2 42.2 %all_gather.18 = bf16[8,2048]{1,0:T(8,128)(2,1)S(1)} all-gather(bf16[8,128]{1,0:T(8,128)(2,1)S(1)} %multiply_convert_fusion.5), channel_id=1, replica_groups=mesh['tp'=16,'dp'=2] {'tp'}, dimensions={1}, use_global_device_ids=true | all-gather | bytes 34816 | tf_op jit(solution)/shard_map/all_gather | solution.py:68
  66.4 35.6 %all_gather.19 = bf16[8,2048]{1,0:T(8,128)(2,1)S(1)} all-gather(bf16[8,128]{1,0:T(8,128)(2,1)S(1)} %multiply_convert_fusion.4), channel_id=1, replica_groups=mesh['tp'=16,'dp'=2] {'tp'}, dimensions={1}, use_global_device_ids=true | all-gather | bytes 34816 | tf_op jit(solution)/shard_map/all_gather | solution.py:69
  102.0 0.2 reshape.108
  102.2 0.3 dynamic-slice_reduce_fusion.1
  102.5 0.2 reshape.107
  102.7 0.2 convert_reduce_fusion.1
  103.0 0.1 multiply_exponential_fusion.1
  103.2 0.7 multiply_reduce_fusion.1
  103.9 0.1 reduce_sum.114
  103.9 0.1 broadcast_multiply_fusion.1
  104.0 4.2 fusion.16
  108.3 0.1 multiply_add_fusion.3
  108.3 0.1 reshape.109
  108.4 0.8 multiply_reduce_fusion.5
  109.3 38.6 %psum.43 = f32[8,16]{1,0:T(8,128)S(1)} all-reduce(f32[8,16]{1,0:T(8,128)S(1)} %broadcast_multiply_fusion.3), channel_id=1, replica_groups=mesh['tp'=16,'dp'=2] {'tp'}, use_global_device_ids=true, to_apply=%region_11.12 | all-reduce | flops 128 | bytes 1024 | tf_op jit(solution)/shard_map/psum | solution.py:95
  147.9 0.1 multiply_reduce_fusion.9
  148.0 0.8 multiply_convert_fusion.1
  148.8 1.8 all_gather.20
  150.6 2.6 fusion.9
  153.4 101.5 %all-reduce.11.cloned.1.call-done = f32[16,2048]{1,0:T(8,128)} async-done(((f32[16,2048]{1,0:T(8,128)}), f32[16,2048]{1,0:T(8,128)}) %all-reduce.11.cloned.1.call-update) | async-done | bytes 131088 | tf_op jit(solution)/shard_map/psum | solution.py:108
  254.8 1.0 fusion.62
  255.9 2.5 psum.45
  258.4 0.2 convolution_convert_fusion.1
  258.6 0.2 convolution_convert_fusion
  258.8 1.3 convolution_convert_fusion.2
  260.1 2.6 fusion.34
  262.8 2.6 fusion.37
  265.4 3.3 all-reduce.6
  268.8 0.6 pad_maximum_fusion.4
  269.5 0.6 pad_maximum_fusion.5
  270.1 38.9 %all_gather.21 = bf16[8,2048]{1,0:T(8,128)(2,1)S(1)} all-gather(bf16[8,128]{1,0:T(8,128)(2,1)S(1)} %multiply_convert_fusion.3), channel_id=1, replica_groups=mesh['tp'=16,'dp'=2] {'tp'}, dimensions={1}, use_global_device_ids=true | all-gather | bytes 34816 | tf_op jit(solution)/shard_map/all_gather | solution.py:68
  308.9 0.2 reshape.110
  309.1 35.6 %all_gather.22 = bf16[8,2048]{1,0:T(8,128)(2,1)S(1)} all-gather(bf16[8,128]{1,0:T(8,128)(2,1)S(1)} %multiply_convert_fusion.2), channel_id=1, replica_groups=mesh['tp'=16,'dp'=2] {'tp'}, dimensions={1}, use_global_device_ids=true | all-gather | bytes 34816 | tf_op jit(solution)/shard_map/all_gather | solution.py:69
  344.8 0.2 reshape.111
  345.0 0.3 dynamic-slice_reduce_fusion
  345.3 0.3 convert_reduce_fusion
  345.6 0.1 multiply_exponential_fusion
  345.7 0.7 multiply_reduce_fusion
  346.4 0.1 reduce_sum.121
  346.5 0.1 broadcast_multiply_fusion
  346.6 4.2 multiply_add_fusion.1
  350.8 2.8 fusion.7
  353.6 0.1 multiply_add_fusion.2
  353.7 0.1 reshape.112
  353.8 0.8 multiply_reduce_fusion.2
  354.7 39.1 %psum.46 = f32[8,16]{1,0:T(8,128)S(1)} all-reduce(f32[8,16]{1,0:T(8,128)S(1)} %broadcast_multiply_fusion.2), channel_id=1, replica_groups=mesh['tp'=16,'dp'=2] {'tp'}, use_global_device_ids=true, to_apply=%region_25.26 | all-reduce | flops 128 | bytes 1024 | tf_op jit(solution)/shard_map/psum | solution.py:95
  393.8 0.1 multiply_reduce_fusion.8
  393.9 0.8 multiply_convert_fusion
  394.7 1.8 all_gather.23
  396.5 2.6 fusion
  399.1 4.1 pad_maximum_fusion
  403.2 0.6 pad_maximum_fusion.1
  403.8 96.8 %all-reduce.13.cloned.1.call-done = f32[16,2048]{1,0:T(8,128)} async-done(((f32[16,2048]{1,0:T(8,128)}), f32[16,2048]{1,0:T(8,128)}) %all-reduce.13.cloned.1.call-update) | async-done | bytes 131088 | tf_op jit(solution)/shard_map/psum | solution.py:108
  500.6 1.6 fusion.65
  (85 shorter events, 0.8 us)
Async XLA Ops:
  7.2 7.5 %copy-start.1 = (bf16[16,2048]{1,0:T(8,128)(2,1)S(1)}, bf16[16,2048]{1,0:T(8,128)(2,1)}, u32[]{:S(2)}) copy-start(bf16[16,2048]{1,0:T(8,128)(2,1)} %param.19) | copy-start | bytes 196612
  7.2 96.0 %reduce-scatter.5.cloned.1.call-start = ((), (), s32[]{:S(2)}) async-start(), calls=%async_computation.4 | async-start | bytes 24576 | tf_op jit(solution)/shard_map/reduce_scatter | solution.py:48
  11.7 5.8 %copy-start.16 = (u32[32]{0:T(128)S(1)}, u32[32]{0:T(128)}, u32[]{:S(2)}) copy-start(u32[32]{0:T(128)} %constant.63) | copy-start | bytes 388
  11.7 7.0 %copy-start.11 = (f32[2,8]{1,0:T(2,128)S(1)}, f32[2,8]{1,0:T(2,128)}, u32[]{:S(2)}) copy-start(f32[2,8]{1,0:T(2,128)} %param.31) | copy-start | bytes 196
  11.7 7.0 %copy-start.9 = (bf16[2,4,128]{2,1,0:T(4,128)(2,1)S(1)}, bf16[2,4,128]{2,1,0:T(4,128)(2,1)}, u32[]{:S(2)}) copy-start(bf16[2,4,128]{2,1,0:T(4,128)(2,1)} %param.27) | copy-start | bytes 6148
  11.7 7.0 %copy-start.10 = (bf16[2,4,128]{2,1,0:T(4,128)(2,1)S(1)}, bf16[2,4,128]{2,1,0:T(4,128)(2,1)}, u32[]{:S(2)}) copy-start(bf16[2,4,128]{2,1,0:T(4,128)(2,1)} %param.28) | copy-start | bytes 6148
  11.7 7.0 %copy-start.8 = (f32[2,512]{1,0:T(2,128)S(1)}, f32[2,512]{1,0:T(2,128)}, u32[]{:S(2)}) copy-start(f32[2,512]{1,0:T(2,128)} %param.32) | copy-start | bytes 12292
  11.7 7.1 %copy-start.5 = (bf16[2,8,3,128]{3,1,2,0:T(8,128)(2,1)S(1)}, bf16[2,8,3,128]{3,1,2,0:T(8,128)(2,1)}, u32[]{:S(2)}) copy-start(bf16[2,8,3,128]{3,1,2,0:T(8,128)(2,1)} %param.35) | copy-start | bytes 36868
  11.7 7.1 %copy-start.6 = (bf16[2,8,3,128]{3,1,2,0:T(8,128)(2,1)S(1)}, bf16[2,8,3,128]{3,1,2,0:T(8,128)(2,1)}, u32[]{:S(2)}) copy-start(bf16[2,8,3,128]{3,1,2,0:T(8,128)(2,1)} %param.36) | copy-start | bytes 36868
  11.7 7.1 %copy-start.14 = (bf16[2,2048,128]{2,1,0:T(8,128)(2,1)S(1)}, bf16[2,2048,128]{2,1,0:T(8,128)(2,1)}, u32[]{:S(2)}) copy-start(bf16[2,2048,128]{2,1,0:T(8,128)(2,1)} %param.23) | copy-start | bytes 3145732
  11.8 7.3 %copy-start.15 = (bf16[2,2048,128]{2,1,0:T(8,128)(2,1)S(1)}, bf16[2,2048,128]{2,1,0:T(8,128)(2,1)}, u32[]{:S(2)}) copy-start(bf16[2,2048,128]{2,1,0:T(8,128)(2,1)} %param.24) | copy-start | bytes 3145732
  14.6 9.5 %copy-start.7 = (bf16[2,4,512]{2,1,0:T(4,128)(2,1)S(1)}, bf16[2,4,512]{2,1,0:T(4,128)(2,1)}, u32[]{:S(2)}) copy-start(bf16[2,4,512]{2,1,0:T(4,128)(2,1)} %param.26) | copy-start | bytes 24580
  14.6 87.4 %copy-start.2 = (bf16[2,8,3,512]{3,1,2,0:T(8,128)(2,1)S(1)}, bf16[2,8,3,512]{3,1,2,0:T(8,128)(2,1)}, u32[]{:S(2)}) copy-start(bf16[2,8,3,512]{3,1,2,0:T(8,128)(2,1)} %param.34) | copy-start | bytes 147460
  14.6 93.8 %reduce-scatter.7.cloned.1.call-start = ((), (), s32[]{:S(2)}) async-start(), calls=%async_computation.5 | async-start | bytes 24576 | tf_op jit(solution)/shard_map/reduce_scatter | solution.py:45
  17.3 85.7 %copy-start.12 = (f32[2,8]{1,0:T(2,128)S(1)}, f32[2,8]{1,0:T(2,128)}, u32[]{:S(2)}) copy-start(f32[2,8]{1,0:T(2,128)} %param.30) | copy-start | bytes 196
  17.3 85.7 %copy-start.13 = (f32[2,8]{1,0:T(2,128)S(1)}, f32[2,8]{1,0:T(2,128)}, u32[]{:S(2)}) copy-start(f32[2,8]{1,0:T(2,128)} %param.29) | copy-start | bytes 196
  17.3 237.5 %all-reduce.11.cloned.1.call-start = ((), (), s32[]{:S(2)}) async-start(), calls=%async_computation.6 | async-start | bytes 262144 | tf_op jit(solution)/shard_map/psum | solution.py:108
  104.0 49.3 %copy-start.3 = (bf16[8,512]{1,0:T(8,128)(2,1)S(1)}, bf16[8,512]{1,0:T(8,128)(2,1)}, u32[]{:S(2)}) copy-start(bf16[8,512]{1,0:T(8,128)(2,1)} %reduce-scatter.5.cloned.1.call-done) | copy-start | bytes 24580
  153.3 192.4 %reduce-scatter.9.cloned.1.call-start = ((), (), s32[]{:S(2)}) async-start(), calls=%async_computation.7 | async-start | bytes 24576 | tf_op jit(solution)/shard_map/reduce_scatter | solution.py:48
  268.8 85.0 %reduce-scatter.11.cloned.1.call-start = ((), (), s32[]{:S(2)}) async-start(), calls=%async_computation.8 | async-start | bytes 24576 | tf_op jit(solution)/shard_map/reduce_scatter | solution.py:45
  345.5 155.1 %all-reduce.13.cloned.1.call-start = ((), (), s32[]{:S(2)}) async-start(), calls=%async_computation.9 | async-start | bytes 262144 | tf_op jit(solution)/shard_map/psum | solution.py:108
  346.6 4.2 copy-start
  399.1 4.1 copy-start.4
Sparse Core Ops, SparseCore 0:
  14.7 10.0 reduce-scatter.4
  27.6 8.6 reduce-scatter.6
  153.4 101.3 all-reduce.10
  268.9 6.5 reduce-scatter.8
  345.7 5.2 reduce-scatter.10
  399.3 101.3 all-reduce.12
where the time goes:
time: 510 us; the launch traced here: 509 us
  blocking collectives  245 us (48%)
  waiting for transfers between devices  198 us (39%)
  matrix products  26.6 us (5%)
  other arithmetic  19.8 us (4%)
  between operations  15.3 us (3%)
    psum x2, waiting for transfers between devices, total_over(): return lax.psum(branch, 'tp')  198 us
    all_gather x2, blocking collectives, mixer_block(): lax.all_gather(write_act.astype(jnp.bfloat16), 'tp', axis=1, tiled=True)  81.1 us
    psum x2, blocking collectives, mixer_block(): lax.psum(jnp.sum(gated_out * gated_out, axis=1)[:, None] * selector[None,...  77.7 us
    all_gather x2, blocking collectives, mixer_block(): lax.all_gather(read_act.astype(jnp.bfloat16), 'tp', axis=1, tiled=True)  71.2 us
    dot_general x10, matrix products, partial_of(): jnp.dot(normed, weight[number], preferred_element_type=jnp.float32)  14.2 us
  transfers between devices with their start and end apart: 6, of which 2 were waited for; matrix products, arithmetic and copies ran while one was open for 5% of the time, Pallas kernels for 0%

commit v1 on v0

--- a/solution.py
+++ b/solution.py
@@ -2,6 +2,7 @@
 import jax.numpy as jnp
 from jax import lax
 from jax.sharding import PartitionSpec as P
+from jax.lax import all_gather
 
 D = 4096
 HEADS = 128
@@ -105,7 +106,7 @@
 
 
 def total_over(branch):
-    return lax.psum(branch, "tp")
+    return jnp.sum(all_gather(branch, axis_name="tp"), axis=0)
 
 
 def local(

time: 510 us -> 420 us (0.82)
  waiting for transfers between devices: 198 us -> 105 us
    psum x2 -> x0, waiting for transfers between devices: 198 us -> none  [total_over(): return lax.psum(branch, 'tp')]
    all_gather x0 -> x2, waiting for transfers between devices: none -> 105 us  [total_over(): return jnp.sum(all_gather(branch, axis_name='tp'), axis=0)]
  transfers between devices with their start and end apart: 6 -> 6, of which waited for: 2 -> 2; matrix products, arithmetic and copies ran while one was open for 5% -> 6% of each run, Pallas kernels for 0% -> 0%
where the time goes in v1:
time: 420 us; the launch traced here: 419 us
  blocking collectives  248 us (59%)
  waiting for transfers between devices  105 us (25%)
  matrix products  28 us (7%)
  other arithmetic  19.2 us (5%)
  between operations  15.3 us (4%)
    all_gather x2, waiting for transfers between devices, total_over(): return jnp.sum(all_gather(branch, axis_name='tp'), axis=0)  105 us
    all_gather x2, blocking collectives, mixer_block(): lax.all_gather(write_act.astype(jnp.bfloat16), 'tp', axis=1, tiled=True)  80.9 us
    psum x2, blocking collectives, mixer_block(): lax.psum(jnp.sum(gated_out * gated_out, axis=1)[:, None] * selector[None,...  80.4 us
    all_gather x2, blocking collectives, mixer_block(): lax.all_gather(read_act.astype(jnp.bfloat16), 'tp', axis=1, tiled=True)  71.2 us
    dot_general x10, matrix products, partial_of(): jnp.dot(normed, weight[number], preferred_element_type=jnp.float32)  14.2 us
    dot_general x2, matrix products, mixer_block(): jnp.einsum('bhpn,bn->bhp', updated, read_vec, precision=lax.Precision.HIG...  8.47 us
  transfers between devices with their start and end apart: 6, of which 2 were waited for; matrix products, arithmetic and copies ran while one was open for 6% of the time, Pallas kernels for 0%

profile of v1, /device:TPU:0, one launch (start us, length us, event | category | flops | bytes accessed | tf_op | source)
XLA Modules:
  0.0 419.0 jit_solution(10809501237007804426)
XLA Ops:
  7.2 1.0 fusion.58
  8.2 2.6 psum.28
  10.8 0.8 fusion.97
  11.8 2.8 fusion.28
  14.7 2.6 fusion.31
  17.4 0.6 dynamic-slice
  18.8 0.2 convolution_convert_fusion.4
  19.1 0.2 convolution_convert_fusion.3
  19.3 1.3 convolution_convert_fusion.5
  20.6 3.5 all-reduce.7
  24.1 42.2 %all_gather.30 = bf16[8,2048]{1,0:T(8,128)(2,1)S(1)} all-gather(bf16[8,128]{1,0:T(8,128)(2,1)S(1)} %multiply_convert_fusion.5), channel_id=1, replica_groups=mesh['tp'=16,'dp'=2] {'tp'}, dimensions={1}, use_global_device_ids=true | all-gather | bytes 34816 | tf_op jit(solution)/shard_map/all_gather | solution.py:69
  66.4 35.6 %all_gather.31 = bf16[8,2048]{1,0:T(8,128)(2,1)S(1)} all-gather(bf16[8,128]{1,0:T(8,128)(2,1)S(1)} %multiply_convert_fusion.4), channel_id=1, replica_groups=mesh['tp'=16,'dp'=2] {'tp'}, dimensions={1}, use_global_device_ids=true | all-gather | bytes 34816 | tf_op jit(solution)/shard_map/all_gather | solution.py:70
  102.0 0.2 reshape.108
  102.2 0.3 dynamic-slice_reduce_fusion.1
  102.5 0.2 reshape.107
  102.7 0.2 convert_reduce_fusion.1
  103.0 0.1 multiply_exponential_fusion.1
  103.1 0.7 multiply_reduce_fusion.1
  103.9 0.1 reduce_sum.132
  103.9 0.1 broadcast_multiply_fusion.1
  104.0 4.2 %fusion.16 = f32[8,1,8,64]{3,1,2,0:T(1,128)S(1)} fusion(bf16[8,128,1,1]{1,2,3,0:T(2,128)(2,1)S(1)} %reshape.128, f32[2,8,8,64,128]{4,3,2,1,0:T(8,128)} %param.37, f32[8,128]{1,0:T(8,128)S(1)} %convert_reduce_fusion.1, f32[8,8,64]{2,1,0:T(8,128)S(1)} %broadcast_multiply_fusion.1, f32[8,8]{1,0:T(8,128)S(1)} %get-tuple-element.27), kind=kOutput, calls=%fused_computation.18 | convolution fusion | flops 7864320 | bytes 2136320 | tf_op jit(solution)/shard_map/bhpn,bn->bhp/dot_general | solution.py:90
  108.2 0.1 multiply_add_fusion.3
  108.3 0.1 reshape.109
  108.4 0.8 multiply_reduce_fusion.5
  109.3 38.6 %psum.29 = f32[8,16]{1,0:T(8,128)S(1)} all-reduce(f32[8,16]{1,0:T(8,128)S(1)} %broadcast_multiply_fusion.3), channel_id=1, replica_groups=mesh['tp'=16,'dp'=2] {'tp'}, use_global_device_ids=true, to_apply=%region_11.12 | all-reduce | flops 128 | bytes 1024 | tf_op jit(solution)/shard_map/psum | solution.py:96
  147.9 0.1 multiply_reduce_fusion.9
  148.0 0.8 multiply_convert_fusion.1
  148.8 1.8 all_gather.32
  150.6 2.6 fusion.9
  153.3 56.4 %all-gather.5.cloned.1.call-done = f32[256,2048]{1,0:T(8,128)} async-done(((f32[16,2048]{1,0:T(8,128)}), f32[256,2048]{1,0:T(8,128)}) %all-gather.5.cloned.1.call-update) | async-done | bytes 2097168 | tf_op jit(solution)/shard_map/all_gather | solution.py:109
  209.7 1.7 reduce_sum.137
  211.4 0.1 fusion.62
  211.5 2.5 psum.30
  214.0 0.2 convolution_convert_fusion.1
  214.3 0.2 convolution_convert_fusion
  214.5 1.3 convolution_convert_fusion.2
  215.8 2.6 fusion.34
  218.4 2.6 fusion.37
  221.0 3.3 all-reduce.6
  224.5 38.6 %all_gather.35 = bf16[8,2048]{1,0:T(8,128)(2,1)S(1)} all-gather(bf16[8,128]{1,0:T(8,128)(2,1)S(1)} %multiply_convert_fusion.3), channel_id=1, replica_groups=mesh['tp'=16,'dp'=2] {'tp'}, dimensions={1}, use_global_device_ids=true | all-gather | bytes 34816 | tf_op jit(solution)/shard_map/all_gather | solution.py:69
  263.1 0.2 reshape.110
  263.3 35.6 %all_gather.36 = bf16[8,2048]{1,0:T(8,128)(2,1)S(1)} all-gather(bf16[8,128]{1,0:T(8,128)(2,1)S(1)} %multiply_convert_fusion.2), channel_id=1, replica_groups=mesh['tp'=16,'dp'=2] {'tp'}, dimensions={1}, use_global_device_ids=true | all-gather | bytes 34816 | tf_op jit(solution)/shard_map/all_gather | solution.py:70
  299.0 0.2 reshape.111
  299.2 0.3 dynamic-slice_reduce_fusion
  299.5 0.3 convert_reduce_fusion
  299.8 0.1 multiply_exponential_fusion
  299.9 0.7 multiply_reduce_fusion
  300.7 0.1 broadcast_multiply_fusion
  300.8 4.2 %fusion.7 = f32[8,1,8,64]{3,1,2,0:T(1,128)S(1)} fusion(bf16[8,128,1,1]{1,2,3,0:T(2,128)(2,1)S(1)} %reshape.130, f32[2,8,8,64,128]{4,3,2,1,0:T(8,128)} %param.37, f32[8,128]{1,0:T(8,128)S(1)} %convert_reduce_fusion, f32[8,8,64]{2,1,0:T(8,128)S(1)} %broadcast_multiply_fusion, f32[8,8]{1,0:T(8,128)S(1)} %get-tuple-element.25), kind=kOutput, calls=%fused_computation.9 | convolution fusion | flops 7864320 | bytes 2136320 | tf_op jit(solution)/shard_map/bhpn,bn->bhp/dot_general | solution.py:90
  305.0 0.1 multiply_add_fusion.2
  305.2 0.8 multiply_reduce_fusion.2
  306.1 41.9 %psum.31 = f32[8,16]{1,0:T(8,128)S(1)} all-reduce(f32[8,16]{1,0:T(8,128)S(1)} %broadcast_multiply_fusion.2), channel_id=1, replica_groups=mesh['tp'=16,'dp'=2] {'tp'}, use_global_device_ids=true, to_apply=%region_25.26 | all-reduce | flops 128 | bytes 1024 | tf_op jit(solution)/shard_map/psum | solution.py:96
  348.0 0.1 multiply_reduce_fusion.8
  348.1 0.8 multiply_convert_fusion
  348.9 1.8 all_gather.37
  350.7 2.6 fusion
  353.4 0.6 pad_maximum_fusion.4
  354.0 0.6 pad_maximum_fusion.5
  354.6 0.6 pad_maximum_fusion.1
  355.2 3.7 multiply_add_fusion.1
  358.9 2.3 pad_maximum_fusion
  361.2 48.5 %all-gather.7.cloned.1.call-done = f32[256,2048]{1,0:T(8,128)} async-done(((f32[16,2048]{1,0:T(8,128)}), f32[256,2048]{1,0:T(8,128)}) %all-gather.7.cloned.1.call-update) | async-done | bytes 2097168 | tf_op jit(solution)/shard_map/all_gather | solution.py:109
  409.8 1.7 reduce_sum.145
  411.5 0.7 fusion.65
  (85 shorter events, 1.0 us)
Async XLA Ops:
  7.2 7.5 %copy-start = (bf16[16,2048]{1,0:T(8,128)(2,1)S(1)}, bf16[16,2048]{1,0:T(8,128)(2,1)}, u32[]{:S(2)}) copy-start(bf16[16,2048]{1,0:T(8,128)(2,1)} %param.19) | copy-start | bytes 196612
  7.2 96.0 %reduce-scatter.5.cloned.1.call-start = ((), (), s32[]{:S(2)}) async-start(), calls=%async_computation.4 | async-start | bytes 24576 | tf_op jit(solution)/shard_map/reduce_scatter | solution.py:49
  11.7 5.8 %copy-start.15 = (u32[32]{0:T(128)S(1)}, u32[32]{0:T(128)}, u32[]{:S(2)}) copy-start(u32[32]{0:T(128)} %constant.63) | copy-start | bytes 388
  11.7 7.0 %copy-start.10 = (f32[2,8]{1,0:T(2,128)S(1)}, f32[2,8]{1,0:T(2,128)}, u32[]{:S(2)}) copy-start(f32[2,8]{1,0:T(2,128)} %param.31) | copy-start | bytes 196
  11.7 7.0 %copy-start.8 = (bf16[2,4,128]{2,1,0:T(4,128)(2,1)S(1)}, bf16[2,4,128]{2,1,0:T(4,128)(2,1)}, u32[]{:S(2)}) copy-start(bf16[2,4,128]{2,1,0:T(4,128)(2,1)} %param.27) | copy-start | bytes 6148
  11.7 7.0 %copy-start.9 = (bf16[2,4,128]{2,1,0:T(4,128)(2,1)S(1)}, bf16[2,4,128]{2,1,0:T(4,128)(2,1)}, u32[]{:S(2)}) copy-start(bf16[2,4,128]{2,1,0:T(4,128)(2,1)} %param.28) | copy-start | bytes 6148
  11.7 7.0 %copy-start.7 = (f32[2,512]{1,0:T(2,128)S(1)}, f32[2,512]{1,0:T(2,128)}, u32[]{:S(2)}) copy-start(f32[2,512]{1,0:T(2,128)} %param.32) | copy-start | bytes 12292
  11.7 7.1 %copy-start.4 = (bf16[2,8,3,128]{3,1,2,0:T(8,128)(2,1)S(1)}, bf16[2,8,3,128]{3,1,2,0:T(8,128)(2,1)}, u32[]{:S(2)}) copy-start(bf16[2,8,3,128]{3,1,2,0:T(8,128)(2,1)} %param.35) | copy-start | bytes 36868
  11.7 7.1 %copy-start.5 = (bf16[2,8,3,128]{3,1,2,0:T(8,128)(2,1)S(1)}, bf16[2,8,3,128]{3,1,2,0:T(8,128)(2,1)}, u32[]{:S(2)}) copy-start(bf16[2,8,3,128]{3,1,2,0:T(8,128)(2,1)} %param.36) | copy-start | bytes 36868
  11.7 7.1 %copy-start.13 = (bf16[2,2048,128]{2,1,0:T(8,128)(2,1)S(1)}, bf16[2,2048,128]{2,1,0:T(8,128)(2,1)}, u32[]{:S(2)}) copy-start(bf16[2,2048,128]{2,1,0:T(8,128)(2,1)} %param.23) | copy-start | bytes 3145732
  11.8 7.3 %copy-start.14 = (bf16[2,2048,128]{2,1,0:T(8,128)(2,1)S(1)}, bf16[2,2048,128]{2,1,0:T(8,128)(2,1)}, u32[]{:S(2)}) copy-start(bf16[2,2048,128]{2,1,0:T(8,128)(2,1)} %param.24) | copy-start | bytes 3145732
  14.6 9.5 %copy-start.6 = (bf16[2,4,512]{2,1,0:T(4,128)(2,1)S(1)}, bf16[2,4,512]{2,1,0:T(4,128)(2,1)}, u32[]{:S(2)}) copy-start(bf16[2,4,512]{2,1,0:T(4,128)(2,1)} %param.26) | copy-start | bytes 24580
  14.6 87.4 %copy-start.1 = (bf16[2,8,3,512]{3,1,2,0:T(8,128)(2,1)S(1)}, bf16[2,8,3,512]{3,1,2,0:T(8,128)(2,1)}, u32[]{:S(2)}) copy-start(bf16[2,8,3,512]{3,1,2,0:T(8,128)(2,1)} %param.34) | copy-start | bytes 147460
  14.6 93.8 %reduce-scatter.7.cloned.1.call-start = ((), (), s32[]{:S(2)}) async-start(), calls=%async_computation.5 | async-start | bytes 24576 | tf_op jit(solution)/shard_map/reduce_scatter | solution.py:46
  17.3 85.7 %copy-start.11 = (f32[2,8]{1,0:T(2,128)S(1)}, f32[2,8]{1,0:T(2,128)}, u32[]{:S(2)}) copy-start(f32[2,8]{1,0:T(2,128)} %param.30) | copy-start | bytes 196
  17.3 85.7 %copy-start.12 = (f32[2,8]{1,0:T(2,128)S(1)}, f32[2,8]{1,0:T(2,128)}, u32[]{:S(2)}) copy-start(f32[2,8]{1,0:T(2,128)} %param.29) | copy-start | bytes 196
  17.3 192.3 %all-gather.5.cloned.1.call-start = ((), (), s32[]{:S(2)}) async-start(), calls=%async_computation.8 | async-start | bytes 2228224 | tf_op jit(solution)/shard_map/all_gather | solution.py:109
  153.2 146.7 %reduce-scatter.9.cloned.1.call-start = ((), (), s32[]{:S(2)}) async-start(), calls=%async_computation.6 | async-start | bytes 24576 | tf_op jit(solution)/shard_map/reduce_scatter | solution.py:49
  224.4 80.8 %reduce-scatter.11.cloned.1.call-start = ((), (), s32[]{:S(2)}) async-start(), calls=%async_computation.7 | async-start | bytes 24576 | tf_op jit(solution)/shard_map/reduce_scatter | solution.py:46
  299.7 110.1 %all-gather.7.cloned.1.call-start = ((), (), s32[]{:S(2)}) async-start(), calls=%async_computation.9 | async-start | bytes 2228224 | tf_op jit(solution)/shard_map/all_gather | solution.py:109
  300.8 52.6 %copy-start.2 = (bf16[8,512]{1,0:T(8,128)(2,1)S(1)}, bf16[8,512]{1,0:T(8,128)(2,1)}, u32[]{:S(2)}) copy-start(bf16[8,512]{1,0:T(8,128)(2,1)} %reduce-scatter.5.cloned.1.call-done) | copy-start | bytes 24580
  300.8 53.8 %copy-start.3 = (bf16[8,512]{1,0:T(8,128)(2,1)S(1)}, bf16[8,512]{1,0:T(8,128)(2,1)}, u32[]{:S(2)}) copy-start(bf16[8,512]{1,0:T(8,128)(2,1)} %reduce-scatter.9.cloned.1.call-done) | copy-start | bytes 24580
Sparse Core Ops, SparseCore 0:
  14.7 10.0 reduce-scatter.4
  27.6 8.6 reduce-scatter.6
  153.3 56.2 all-gather.4
  224.6 6.2 reduce-scatter.8
  299.9 5.2 reduce-scatter.10
  353.5 56.2 all-gather.6
